TPU v7x, 32 devices: a whole 2x2x4 slice. The times are simulated.
32 devices in a mesh: sp: 8 (over z, y), tp: 4 (over x, core).
Axes of the slice: x: 2, y: 2, z: 4, core: 2. Of those that a mesh axis runs over, the one named last changes fastest.
Arguments:
- stream: bfloat16 [3072, 2048], P(('sp', 'tp')), may hold values from -6 to 6
- query_projected: bfloat16 [3072, 1024], P('sp', 'tp'), may hold values from -6 to 6
- key_projected: bfloat16 [3072, 1024], P('sp', 'tp'), may hold values from -6 to 6
- value_projected: bfloat16 [3072, 1024], P('sp', 'tp'), may hold values from -6 to 6
- gate_projected: bfloat16 [3072, 1024], P('sp', 'tp'), may hold values from -6 to 6
- strength_logits: bfloat16 [8, 3072], P('tp', 'sp'), may hold values from -7 to 4
- decay_preactivation: bfloat16 [8, 3072], P('tp', 'sp'), may hold values from -9 to 9
- extra_log_decay: float32 [8, 3072], P('tp', 'sp'), may hold values from -0.7 to 0
- head_decay_rate: float32 [8], P('tp'), may hold values from 0 to 0.1
- head_norm_gain: float32 [128], replicated, may hold values from 0.1 to 1.9
- head_output_matrix: bfloat16 [1024, 2048], P('tp'), may hold values from -0.1875 to 0.1875
- feed_norm_gain: float32 [2048], replicated, may hold values from 0.1 to 1.9
- gate_matrix: bfloat16 [2048, 5632], P('sp', 'tp'), may hold values from -0.125 to 0.125
- up_matrix: bfloat16 [2048, 5632], P('sp', 'tp'), may hold values from -0.125 to 0.125
- down_matrix: bfloat16 [5632, 2048], P('tp', 'sp'), may hold values from -0.078125 to 0.078125
Outputs:
- result: bfloat16 [3072, 2048], P(('sp', 'tp'))
All inputs are finite; a program needn't handle non-finite values.
Results may differ from a plain program's by a relative error of at most 0.015.
Values may be sent and summed in bfloat16 or wider, within the bound.
No kernel may reach another device: no remote copies, remote signals or barrier semaphores. Data moves between devices by JAX's collectives and lax.ppermute only.
A program may use at most 128 MiB of HBM per device.

v0:
```python
import jax
import jax.numpy as jnp
from jax import lax
from jax.sharding import PartitionSpec as P

HEAD = 128
BLOCK = 64
PRECISION_FULL = lax.Precision.HIGHEST
EPSILON = 1e-06


def from_behind(value, axis, by):
    size = lax.axis_size(axis)
    pairs = [(i, i + by) for i in range(size) if 0 <= i + by < size]
    return lax.ppermute(value, axis, pairs)


def unit_rows(tensor):
    return tensor * lax.rsqrt(jnp.sum(tensor * tensor, axis=-1, keepdims=True) + EPSILON)


def rms_scale(tensor):
    return tensor * lax.rsqrt(jnp.mean(tensor * tensor, axis=-1, keepdims=True) + EPSILON)


def unit_lower_inverse(strict_lower):
    size = strict_lower.shape[-1]
    row = jnp.arange(size)[:, None]
    column = jnp.arange(size)[None, :]

    def corner(half):
        same_pair = row // (2 * half) == column // (2 * half)
        return jnp.where(same_pair & (row // half != column // half), strict_lower, 0.0)

    inverse = jnp.eye(size, dtype=jnp.float32) - corner(1)
    half = 2
    while half < size:
        left = jnp.einsum("hnij,hnjk->hnik", inverse, corner(half), precision=PRECISION_FULL)
        inverse = inverse - jnp.einsum("hnij,hnjk->hnik", left, inverse, precision=PRECISION_FULL)
        half *= 2
    return inverse


def swap(value, axis, bit):
    size = lax.axis_size(axis)
    return lax.ppermute(value, axis, [(i, i ^ bit) for i in range(size)])


def relative_order(count):
    order = [0]
    bit = count // 2
    while bit:
        order = order + [place ^ bit for place in order]
        bit //= 2
    return order


def gather_relative(own):
    bit = lax.axis_size("tp") // 2
    while bit:
        own = jnp.concatenate([own, swap(own, "tp", bit)], axis=0)
        bit //= 2
    return own


def scatter_relative(left_rows, matrix):
    size = lax.axis_size("tp")
    if size == 1:
        return jnp.dot(left_rows, matrix, preferred_element_type=jnp.float32)
    half = left_rows.shape[0] // 2
    leaving = jnp.dot(left_rows[half:], matrix, preferred_element_type=jnp.float32)
    arrived = swap(leaving.astype(jnp.bfloat16), "tp", 1)
    total = jnp.dot(left_rows[:half], matrix, preferred_element_type=jnp.float32)
    total = total + arrived.astype(jnp.float32)
    bit = 2
    while bit < size:
        half = total.shape[0] // 2
        arrived = swap(total[half:].astype(jnp.bfloat16), "tp", bit)
        total = total[:half] + arrived.astype(jnp.float32)
        bit *= 2
    return total


def inflow_of_earlier(matrix_product, running_state):
    size = lax.axis_size("sp")
    width = running_state.shape[-1]
    pair = jnp.concatenate([matrix_product, running_state], axis=-1)
    pair = from_behind(pair.astype(jnp.bfloat16), "sp", 1).astype(jnp.float32)
    by = 1
    while by < size - 1:
        matrix, state = (pair[..., :width], pair[..., width:])
        last = 2 * by >= size - 1
        sent = (state if last else pair).astype(jnp.bfloat16)
        earlier = from_behind(sent, "sp", by).astype(jnp.float32)
        moved = jnp.einsum("hij,hjk->hik", matrix, earlier, precision=PRECISION_FULL)
        if last:
            pair = jnp.concatenate([matrix, state + moved], axis=-1)
        else:
            pair = jnp.concatenate([moved[..., :width], state + moved[..., width:]], axis=-1)
        by *= 2
    return pair[..., width:]


def block_correction(
    unit_queries,
    unit_keys,
    complete_values,
    strength_logits,
    decay_preactivation,
    extra_log_decay,
    head_decay_rate,
):
    head_count, length, head_width = unit_queries.shape
    block_count = length // BLOCK

    def to_blocks(tensor):
        return tensor.reshape((head_count, block_count, BLOCK) + tensor.shape[2:])

    beta_gate = jax.nn.sigmoid(strength_logits.astype(jnp.float32))
    decay_logarithm = (
        -head_decay_rate[:, None] * jax.nn.softplus(decay_preactivation.astype(jnp.float32))
        + extra_log_decay
    )
    query_block = to_blocks(unit_queries)
    key_block = to_blocks(unit_keys)
    value_block = to_blocks(complete_values)
    beta_block = to_blocks(beta_gate)
    cumulative = jnp.cumsum(to_blocks(decay_logarithm), axis=-1)
    causal = jnp.tril(jnp.ones((BLOCK, BLOCK), bool))
    strict = jnp.tril(jnp.ones((BLOCK, BLOCK), bool), -1)
    spread = cumulative[..., :, None] - cumulative[..., None, :]
    damping = jnp.where(causal, jnp.exp(jnp.where(causal, spread, 0.0)), 0.0)
    key_beta = key_block * beta_block[..., None]
    lower_part = jnp.einsum(
        "hnid,hnjd->hnij", key_beta, key_block, precision=PRECISION_FULL
    ) * jnp.where(strict, damping, 0.0)
    right_side = jnp.concatenate(
        [value_block * beta_block[..., None], key_beta * jnp.exp(cumulative)[..., None]], axis=-1
    )
    solved = jnp.einsum(
        "hnij,hnjd->hnid", unit_lower_inverse(lower_part), right_side, precision=PRECISION_FULL
    )
    target_values = solved[..., :head_width]
    householder_weights = solved[..., head_width:]
    inner_scores = (
        jnp.einsum("hnid,hnjd->hnij", query_block, key_block, precision=PRECISION_FULL) * damping
    )
    decayed_queries = query_block * jnp.exp(cumulative)[..., None]
    closing_log_decay = cumulative[..., -1:]
    decayed_keys = key_block * jnp.exp(closing_log_decay - cumulative)[..., None]
    return (
        decayed_queries,
        decayed_keys,
        target_values,
        householder_weights,
        inner_scores,
        closing_log_decay,
    )


def local_recurrence(
    query_projected,
    key_projected,
    value_projected,
    strength_logits,
    decay_preactivation,
    extra_log_decay,
    head_decay_rate,
):
    head_count = strength_logits.shape[0]
    tok_count = strength_logits.shape[1]

    def split_heads(tensor):
        return tensor.reshape(tok_count, head_count, HEAD).transpose(1, 0, 2).astype(jnp.float32)

    unit_queries = unit_rows(split_heads(query_projected)) * HEAD ** (-0.5)
    unit_keys = unit_rows(split_heads(key_projected))
    complete_values = split_heads(value_projected)
    score_terms = block_correction(
        unit_queries,
        unit_keys,
        complete_values,
        strength_logits,
        decay_preactivation,
        extra_log_decay,
        head_decay_rate,
    )
    identity = jnp.broadcast_to(jnp.eye(HEAD, dtype=jnp.float32), (head_count, HEAD, HEAD))

    def advance(carry, items):
        running_state, matrix_product = carry
        (
            decayed_queries,
            decayed_keys,
            target_values,
            householder_weights,
            inner_scores,
            closing_log_decay,
        ) = items
        new_state = target_values - jnp.einsum(
            "fdc,fcj->fdj", householder_weights, running_state, precision=PRECISION_FULL
        )
        layer_output = jnp.einsum(
            "fdc,fcj->fdj", decayed_queries, running_state, precision=PRECISION_FULL
        )
        layer_output = layer_output + jnp.einsum(
            "hij,hjv->hiv", inner_scores, new_state, precision=PRECISION_FULL
        )
        passed_state = decayed_queries - jnp.einsum(
            "hij,hjk->hik", inner_scores, householder_weights, precision=PRECISION_FULL
        )
        decay_span = jnp.einsum(
            "fdc,fcj->fdj", passed_state, matrix_product, precision=PRECISION_FULL
        )
        decay_factor = jnp.exp(closing_log_decay)[:, :, None]
        step_map = decay_factor * identity - jnp.einsum(
            "hik,hij->hkj", decayed_keys, householder_weights, precision=PRECISION_FULL
        )
        running_state = decay_factor * running_state + jnp.einsum(
            "xwp,xws->xps", decayed_keys, new_state, precision=PRECISION_FULL
        )
        matrix_product = jnp.einsum(
            "hij,hjk->hik", step_map, matrix_product, precision=PRECISION_FULL
        )
        return ((running_state, matrix_product), (layer_output, decay_span))

    moved = tuple((jnp.moveaxis(tensor, 1, 0) for tensor in score_terms))
    zeros_state = jnp.zeros((head_count, HEAD, HEAD), jnp.float32)
    (running_state, matrix_product), (block_outputs, decay_spans) = lax.scan(
        advance, (zeros_state, identity), moved
    )

    def merge_blocks(tensor):
        return jnp.moveaxis(tensor, 0, 1).reshape(head_count, tok_count, HEAD)

    return (
        merge_blocks(block_outputs),
        merge_blocks(decay_spans),
        matrix_product,
        running_state,
        identity,
    )


def body(
    stream,
    query_projected,
    key_projected,
    value_projected,
    gate_projected,
    strength_logits,
    decay_preactivation,
    extra_log_decay,
    head_decay_rate,
    head_norm_gain,
    head_output_matrix,
    feed_norm_gain,
    gate_matrix,
    up_matrix,
    down_matrix,
):
    gate_whole = lax.all_gather(gate_matrix, "sp", axis=0, tiled=True)
    up_whole = lax.all_gather(up_matrix, "sp", axis=0, tiled=True)
    down_whole = lax.all_gather(down_matrix, "sp", axis=1, tiled=True)
    block_outputs, decay_spans, matrix_product, running_state, _ = local_recurrence(
        query_projected,
        key_projected,
        value_projected,
        strength_logits,
        decay_preactivation,
        extra_log_decay,
        head_decay_rate,
    )
    state_inflow = inflow_of_earlier(matrix_product, running_state)
    attention_output = block_outputs + jnp.einsum(
        "qwc,qcn->qwn", decay_spans, state_inflow, precision=PRECISION_FULL
    )
    head_count = attention_output.shape[0]
    tok_count = attention_output.shape[1]
    normed_heads = rms_scale(attention_output) * head_norm_gain
    gated = normed_heads.transpose(1, 0, 2).reshape(tok_count, head_count * HEAD)
    mixed = (gated * jax.nn.silu(gate_projected.astype(jnp.float32))).astype(jnp.bfloat16)
    tp_size = lax.axis_size("tp")
    tp_index = lax.axis_index("tp")
    chunks = mixed.reshape(tp_size, tok_count // tp_size, head_count * HEAD)
    ordered = jnp.concatenate(
        [
            lax.dynamic_index_in_dim(chunks, tp_index ^ place, 0, keepdims=False)
            for place in relative_order(tp_size)
        ],
        axis=0,
    )
    branch = scatter_relative(ordered, head_output_matrix)
    residual_own = stream.astype(jnp.float32) + branch
    normed_own = (rms_scale(residual_own) * feed_norm_gain).astype(jnp.bfloat16)
    whole_rows = gather_relative(normed_own)
    gate_total = jnp.dot(whole_rows, gate_whole, preferred_element_type=jnp.float32)
    up_total = jnp.dot(whole_rows, up_whole, preferred_element_type=jnp.float32)
    hidden = (jax.nn.silu(gate_total) * up_total).astype(jnp.bfloat16)
    ffn_own = scatter_relative(hidden, down_whole)
    return (residual_own + ffn_own).astype(jnp.bfloat16)


def solution(mesh):
    placed = (
        P(("sp", "tp"), None),
        P("sp", "tp"),
        P("sp", "tp"),
        P("sp", "tp"),
        P("sp", "tp"),
        P("tp", "sp"),
        P("tp", "sp"),
        P("tp", "sp"),
        P("tp"),
        P(),
        P("tp", None),
        P(),
        P("sp", "tp"),
        P("sp", "tp"),
        P("tp", "sp"),
    )
    return jax.shard_map(
        body, mesh=mesh, in_specs=placed, out_specs=P(("sp", "tp"), None), check_vma=False
    )
```

profile of v0, /device:TPU:0, one launch (start us, length us, event | category | flops | bytes accessed | tf_op | source)
XLA Modules:
  0.0 326.3 jit_solution(2462705551969413879)
XLA Ops:
  20.0 26.2 %while.17 = (s32[]{:T(128)}, f32[2,128,128]{2,1,0:T(8,128)S(1)}, f32[2,128,128]{2,1,0:T(8,128)S(1)}, f32[6,2,64,128]{3,2,0,1:T(8,128)}, f32[6,2,64,128]{3,2,0,1:...) while((s32[]{:T(128)}, f32[2,128,128]{2,1,0:T(8,128)S(1)}, ...), condition=%wide.region_4.5_spmd.clone, body=%wide.region_3.4_spmd.clone.sunk | while | flops 201605120 | bytes 2758829 | solution.py:229
  20.0 1.1 convolution_subtract_fusion.11
  24.4 1.1 convolution_subtract_fusion.11
  27.2 0.9 fusion.206
  28.7 1.1 convolution_subtract_fusion.11
  31.6 0.9 fusion.206
  33.1 1.1 convolution_subtract_fusion.11
  37.5 1.1 convolution_subtract_fusion.11
  41.8 1.1 convolution_subtract_fusion.11
  44.7 0.9 fusion.206
  46.3 5.0 %collective-permute-start = (bf16[2,128,256]{2,1,0:T(8,128)(2,1)S(1)}, bf16[2,128,256]{2,1,0:T(8,128)(2,1)S(1)}, u32[]{:S(2)}, u32[]{:S(2)}) collective-permute-start(bf16[2,128,256]{2,1,0:T(8,128)(2,1)S(1)} %pad_maximum_fusion.6), channel_id=1, source_target_pairs={{0,4},{4,8},{8,12},{12,16},{16,20},{20,24},{24,28},{1,5},{5,9},{9,... | collective-permute-start | bytes 393224 | tf_op jit(solution)/shard_map/ppermute | solution.py:15
  51.3 5.5 %collective-permute-done = bf16[2,128,256]{2,1,0:T(8,128)(2,1)S(1)} collective-permute-done((bf16[2,128,256]{2,1,0:T(8,128)(2,1)S(1)}, bf16[2,128,256]{2,1,0:T(8,128)(2,1)S(1)}, u32[]{:S(2)}, u32[]{:S(2)}) %collective-permute-start) | collective-permute-done | bytes 131104 | tf_op jit(solution)/shard_map/ppermute | solution.py:15
  56.9 4.4 %collective-permute-start.1 = (bf16[2,128,256]{2,1,0:T(8,128)(2,1)S(1)}, bf16[2,128,256]{2,1,0:T(8,128)(2,1)S(1)}, u32[]{:S(2)}, u32[]{:S(2)}) collective-permute-start(bf16[2,128,256]{2,1,0:T(8,128)(2,1)S(1)} %collective-permute-done), channel_id=1, source_target_pairs={{0,4},{4,8},{8,12},{12,16},{16,20},{20,24},{24,28},{1,5},{5,9},{9,... | collective-permute-start | bytes 393224 | tf_op jit(solution)/shard_map/ppermute | solution.py:15
  61.2 5.4 %collective-permute-done.1 = bf16[2,128,256]{2,1,0:T(8,128)(2,1)S(1)} collective-permute-done((bf16[2,128,256]{2,1,0:T(8,128)(2,1)S(1)}, bf16[2,128,256]{2,1,0:T(8,128)(2,1)S(1)}, u32[]{:S(2)}, u32[]{:S(2)}) %collective-permute-start.1) | collective-permute-done | bytes 131104 | tf_op jit(solution)/shard_map/ppermute | solution.py:15
  66.9 6.0 %collective-permute-start.2 = (bf16[2,128,256]{2,1,0:T(8,128)(2,1)S(1)}, bf16[2,128,256]{2,1,0:T(8,128)(2,1)S(1)}, u32[]{:S(2)}, u32[]{:S(2)}) collective-permute-start(bf16[2,128,256]{2,1,0:T(8,128)(2,1)S(1)} %pad_maximum_fusion.7), channel_id=1, source_target_pairs={{0,8},{4,12},{8,16},{12,20},{16,24},{20,28},{1,9},{5,13},{9,17},{1... | collective-permute-start | bytes 393224 | tf_op jit(solution)/shard_map/ppermute | solution.py:15
  72.9 5.4 %collective-permute-done.2 = bf16[2,128,256]{2,1,0:T(8,128)(2,1)S(1)} collective-permute-done((bf16[2,128,256]{2,1,0:T(8,128)(2,1)S(1)}, bf16[2,128,256]{2,1,0:T(8,128)(2,1)S(1)}, u32[]{:S(2)}, u32[]{:S(2)}) %collective-permute-start.2) | collective-permute-done | bytes 131104 | tf_op jit(solution)/shard_map/ppermute | solution.py:15
  78.6 20.5 %collective-permute-start.3 = (bf16[2,128,128]{2,1,0:T(8,128)(2,1)S(1)}, bf16[2,128,128]{2,1,0:T(8,128)(2,1)S(1)}, u32[]{:S(2)}, u32[]{:S(2)}) collective-permute-start(bf16[2,128,128]{2,1,0:T(8,128)(2,1)S(1)} %fusion.128), channel_id=1, source_target_pairs={{0,16},{4,20},{8,24},{12,28},{1,17},{5,21},{9,25},{13,29},{2,18},{... | collective-permute-start | bytes 196616 | tf_op jit(solution)/shard_map/ppermute | solution.py:15
  99.3 2.9 collective-permute-done.3
  104.1 2.3 collective-permute-done.4
  106.9 11.1 %collective-permute-done.5 = bf16[96,2048]{1,0:T(8,128)(2,1)S(1)} collective-permute-done((bf16[96,2048]{1,0:T(8,128)(2,1)S(1)}, bf16[96,2048]{1,0:T(8,128)(2,1)S(1)}, u32[]{:S(2)}, u32[]{:S(2)}) %collective-permute-start.5) | collective-permute-done | bytes 393248 | tf_op jit(solution)/shard_map/ppermute | solution.py:46
  118.8 10.0 %collective-permute-done.6 = bf16[96,2048]{1,0:T(8,128)(2,1)S(1)} collective-permute-done((bf16[96,2048]{1,0:T(8,128)(2,1)S(1)}, bf16[96,2048]{1,0:T(8,128)(2,1)S(1)}, u32[]{:S(2)}, u32[]{:S(2)}) %collective-permute-start.6) | collective-permute-done | bytes 393248 | tf_op jit(solution)/shard_map/ppermute | solution.py:46
  129.6 1.8 collective-permute-done.7
  131.4 7.1 %fusion.47 = f32[384,1408]{1,0:T(8,128)} fusion(bf16[2048,1408]{1,0:T(8,128)(2,1)} %all-gather.4.cloned.1.call-done, bf16[192,2048]{1,0:T(8,128)(2,1)} %collective-permute-done.7, bf16[96,2048]{1,0:T(8,128)(2,1)} %copy-done.7, bf16[96,2048]{1,0:T(8,128)(2,1)} %copy-done.2), kind=kOutput, calls=%fused_computation.75 | convolution fusion | flops 2219311104 | bytes 9502720 | tf_op jit(solution)/shard_map/dot_general | solution.py:297
  138.5 67.4 %all-gather.6.cloned.1.call-done = bf16[2048,1408]{1,0:T(8,128)(2,1)} async-done(((bf16[256,1408]{1,0:T(8,128)(2,1)}), bf16[2048,1408]{1,0:T(8,128)(2,1)}) %all-gather.6.cloned.1.call-update) | async-done | bytes 5767184 | tf_op jit(solution)/shard_map/all_gather | solution.py:263
  206.0 7.4 %multiply_convert_fusion = bf16[384,1408]{1,0:T(8,128)(2,1)} fusion(f32[384,1408]{1,0:T(8,128)} %fusion.47, bf16[2048,1408]{1,0:T(8,128)(2,1)} %all-gather.6.cloned.1.call-done, bf16[192,2048]{1,0:T(8,128)(2,1)} %collective-permute-done.7, bf16[96,2048]{1,0:T(8,128)(2,1)} %copy-done.7, bf16[96,2048]{1,0:T(8,128)(2,1)} %copy-done.2), kind=kOutput, calls=%fused_computation.46 | convolution fusion | flops 2222555136 | bytes 10584064 | tf_op jit(solution)/shard_map/dot_general | solution.py:298
  213.4 86.0 %all-gather.8.cloned.1.call-done = bf16[1408,2048]{1,0:T(8,128)(2,1)} async-done(((bf16[1408,256]{1,0:T(8,128)(2,1)}), bf16[1408,2048]{1,0:T(8,128)(2,1)}) %all-gather.8.cloned.1.call-update) | async-done | bytes 5767184 | tf_op jit(solution)/shard_map/all_gather | solution.py:264
  299.4 4.3 %convolution_convert_fusion = bf16[192,2048]{1,0:T(8,128)(2,1)S(1)} fusion(bf16[1408,2048]{1,0:T(8,128)(2,1)} %all-gather.8.cloned.1.call-done, bf16[384,1408]{1,0:T(8,128)(2,1)} %multiply_convert_fusion), kind=kOutput, calls=%fused_computation.44 | convolution fusion | flops 1107689472 | bytes 7094272 | tf_op jit(solution)/shard_map/dot_general | solution.py:71
  303.8 2.3 collective-permute-done.8
  306.1 1.4 convert_add_fusion
  307.5 1.6 collective-permute-start.9
  309.1 9.6 %collective-permute-done.9 = bf16[96,2048]{1,0:T(8,128)(2,1)S(1)} collective-permute-done((bf16[96,2048]{1,0:T(8,128)(2,1)S(1)}, bf16[96,2048]{1,0:T(8,128)(2,1)S(1)}, u32[]{:S(2)}, u32[]{:S(2)}) %collective-permute-start.9) | collective-permute-done | bytes 393248 | tf_op jit(solution)/shard_map/ppermute | solution.py:46
  318.7 1.0 fusion.40
  (167 shorter events, 34.4 us)
Async XLA Ops:
  6.5 97.1 %copy-start = (bf16[256,2048]{1,0:T(8,128)(2,1)S(1)}, bf16[256,2048]{1,0:T(8,128)(2,1)}, u32[]{:S(2)}) copy-start(bf16[256,2048]{1,0:T(8,128)(2,1)} %param.27) | copy-start | bytes 3145732
  6.5 2.3 copy-start.16
  6.5 2.4 copy-start.12
  6.5 2.4 copy-start.11
  6.5 2.5 copy-start.3
  6.5 3.0 copy-start.13
  6.6 124.9 %all-gather.4.cloned.1.call-start = ((), (), s32[]{:S(2)}) async-start(), calls=%async_computation | async-start | bytes 6488064 | tf_op jit(solution)/shard_map/all_gather | solution.py:262
  7.3 198.7 %all-gather.6.cloned.1.call-start = ((), (), s32[]{:S(2)}) async-start(), calls=%async_computation.1 | async-start | bytes 6488064 | tf_op jit(solution)/shard_map/all_gather | solution.py:263
  8.0 291.3 %all-gather.8.cloned.1.call-start = ((), (), s32[]{:S(2)}) async-start(), calls=%async_computation.2 | async-start | bytes 6488064 | tf_op jit(solution)/shard_map/all_gather | solution.py:264
  14.4 2.3 copy-start.4
  14.9 2.1 copy-start.8
  46.2 52.9 %copy-start.5 = (f32[6,2,64,128]{3,2,0,1:T(8,128)S(1)}, f32[6,2,64,128]{3,2,0,1:T(8,128)}, u32[]{:S(2)}) copy-start(f32[6,2,64,128]{3,2,0,1:T(8,128)} %get-tuple-element.70) | copy-start | bytes 1179652
  46.2 56.2 %copy-start.6 = (f32[6,2,64,128]{3,2,0,1:T(8,128)S(1)}, f32[6,2,64,128]{3,2,0,1:T(8,128)}, u32[]{:S(2)}) copy-start(f32[6,2,64,128]{3,2,0,1:T(8,128)} %get-tuple-element.71) | copy-start | bytes 1179652
  46.3 10.6 %collective-permute-start = (bf16[2,128,256]{2,1,0:T(8,128)(2,1)S(1)}, bf16[2,128,256]{2,1,0:T(8,128)(2,1)S(1)}, u32[]{:S(2)}, u32[]{:S(2)}) collective-permute-start(bf16[2,128,256]{2,1,0:T(8,128)(2,1)S(1)} %pad_maximum_fusion.6), channel_id=1, source_target_pairs={{0,4},{4,8},{8,12},{12,16},{16,20},{20,24},{24,28},{1,5},{5,9},{9,... | collective-permute-start | bytes 393224 | tf_op jit(solution)/shard_map/ppermute | solution.py:15
  56.9 9.8 %collective-permute-start.1 = (bf16[2,128,256]{2,1,0:T(8,128)(2,1)S(1)}, bf16[2,128,256]{2,1,0:T(8,128)(2,1)S(1)}, u32[]{:S(2)}, u32[]{:S(2)}) collective-permute-start(bf16[2,128,256]{2,1,0:T(8,128)(2,1)S(1)} %collective-permute-done), channel_id=1, source_target_pairs={{0,4},{4,8},{8,12},{12,16},{16,20},{20,24},{24,28},{1,5},{5,9},{9,... | collective-permute-start | bytes 393224 | tf_op jit(solution)/shard_map/ppermute | solution.py:15
  66.8 36.3 %copy-start.14 = (f32[128]{0:T(128)S(1)}, f32[128]{0:T(128)}, u32[]{:S(2)}) copy-start(f32[128]{0:T(128)} %param.26) | copy-start | bytes 1540
  66.9 11.4 %collective-permute-start.2 = (bf16[2,128,256]{2,1,0:T(8,128)(2,1)S(1)}, bf16[2,128,256]{2,1,0:T(8,128)(2,1)S(1)}, u32[]{:S(2)}, u32[]{:S(2)}) collective-permute-start(bf16[2,128,256]{2,1,0:T(8,128)(2,1)S(1)} %pad_maximum_fusion.7), channel_id=1, source_target_pairs={{0,8},{4,12},{8,16},{12,20},{16,24},{20,28},{1,9},{5,13},{9,17},{1... | collective-permute-start | bytes 393224 | tf_op jit(solution)/shard_map/ppermute | solution.py:15
  78.6 24.8 %copy-start.9 = (bf16[384,256]{1,0:T(8,128)(2,1)S(1)}, bf16[384,256]{1,0:T(8,128)(2,1)}, u32[]{:S(2)}) copy-start(bf16[384,256]{1,0:T(8,128)(2,1)} %param.21) | copy-start | bytes 589828
  78.6 23.6 %collective-permute-start.3 = (bf16[2,128,128]{2,1,0:T(8,128)(2,1)S(1)}, bf16[2,128,128]{2,1,0:T(8,128)(2,1)S(1)}, u32[]{:S(2)}, u32[]{:S(2)}) collective-permute-start(bf16[2,128,128]{2,1,0:T(8,128)(2,1)S(1)} %fusion.128), channel_id=1, source_target_pairs={{0,16},{4,20},{8,24},{12,28},{1,17},{5,21},{9,25},{13,29},{2,18},{... | collective-permute-start | bytes 196616 | tf_op jit(solution)/shard_map/ppermute | solution.py:15
  104.0 14.0 %copy-start.1 = (bf16[96,2048]{1,0:T(8,128)(2,1)S(1)}, bf16[96,2048]{1,0:T(8,128)(2,1)}, u32[]{:S(2)}) copy-start(bf16[96,2048]{1,0:T(8,128)(2,1)} %param.17) | copy-start | bytes 1179652
  104.0 2.4 collective-permute-start.4
  106.3 11.9 %copy-start.10 = (f32[2048]{0:T(1024)S(1)}, f32[2048]{0:T(1024)}, u32[]{:S(2)}) copy-start(f32[2048]{0:T(1024)} %param.28) | copy-start | bytes 24580
  106.8 11.2 %collective-permute-start.5 = (bf16[96,2048]{1,0:T(8,128)(2,1)S(1)}, bf16[96,2048]{1,0:T(8,128)(2,1)S(1)}, u32[]{:S(2)}, u32[]{:S(2)}) collective-permute-start(bf16[96,2048]{1,0:T(8,128)(2,1)S(1)} %slice.148), channel_id=1, source_target_pairs={{0,2},{1,3},{2,0},{3,1},{4,6},{5,7},{6,4},{7,5},{8,10},{9,11},{10,... | collective-permute-start | bytes 1179656 | tf_op jit(solution)/shard_map/ppermute | solution.py:46
  118.5 10.4 %copy-start.2 = (bf16[96,2048]{1,0:T(8,128)(2,1)}, bf16[96,2048]{1,0:T(8,128)(2,1)S(1)}, u32[]{:S(2)}) copy-start(bf16[96,2048]{1,0:T(8,128)(2,1)S(1)} %multiply_convert_fusion.1) | copy-start | bytes 1179652
  118.5 10.4 %collective-permute-start.6 = (bf16[96,2048]{1,0:T(8,128)(2,1)S(1)}, bf16[96,2048]{1,0:T(8,128)(2,1)S(1)}, u32[]{:S(2)}, u32[]{:S(2)}) collective-permute-start(bf16[96,2048]{1,0:T(8,128)(2,1)S(1)} %multiply_convert_fusion.1), channel_id=1, source_target_pairs={{0,2},{1,3},{2,0},{3,1},{4,6},{5,7},{6,4},{7,5},{8,10},{9,11},{10,... | collective-permute-start | bytes 1179656 | tf_op jit(solution)/shard_map/ppermute | solution.py:46
  128.9 0.7 copy-start.7
  128.9 2.5 collective-permute-start.7
  299.4 6.7 %copy-start.15 = (bf16[1408,2048]{1,0:T(8,128)(2,1)S(1)}, bf16[1408,2048]{1,0:T(8,128)(2,1)}, u32[]{:S(2)}) copy-start(bf16[1408,2048]{1,0:T(8,128)(2,1)} %all-gather.8.cloned.1.call-done) | copy-start | bytes 17301508
  299.4 6.7 %copy-start.17 = (bf16[384,1408]{1,0:T(8,128)(2,1)S(1)}, bf16[384,1408]{1,0:T(8,128)(2,1)}, u32[]{:S(2)}) copy-start(bf16[384,1408]{1,0:T(8,128)(2,1)} %multiply_convert_fusion) | copy-start | bytes 3244036
  303.7 2.4 collective-permute-start.8
  307.5 11.2 %collective-permute-start.9 = (bf16[96,2048]{1,0:T(8,128)(2,1)S(1)}, bf16[96,2048]{1,0:T(8,128)(2,1)S(1)}, u32[]{:S(2)}, u32[]{:S(2)}) collective-permute-start(bf16[96,2048]{1,0:T(8,128)(2,1)S(1)} %slice.147), channel_id=1, source_target_pairs={{0,2},{1,3},{2,0},{3,1},{4,6},{5,7},{6,4},{7,5},{8,10},{9,11},{10,... | collective-permute-start | bytes 1179656 | tf_op jit(solution)/shard_map/ppermute | solution.py:46
Sparse Core Ops, SparseCore 0:
  9.5 99.7 all-gather.3
  111.5 94.4 all-gather.5
  208.0 91.2 all-gather.7
where the time goes:
time: 327 us; the launch traced here: 326 us
  waiting for transfers between devices  212 us (65%)
  matrix products  55.6 us (17%)
  starting transfers between devices  38.3 us (12%)
  between operations  13.8 us (4%)
  other arithmetic  3.82 us (1%)
    all_gather x1, waiting for transfers between devices, body(): down_whole = lax.all_gather(down_matrix, 'sp', axis=1, tiled=True)  86 us
    all_gather x1, waiting for transfers between devices, body(): up_whole = lax.all_gather(up_matrix, 'sp', axis=0, tiled=True)  67.4 us
    ppermute x6, waiting for transfers between devices, swap(): return lax.ppermute(value, axis, [(i, i ^ bit) for i in range(size)])  37.2 us
    ppermute x4, starting transfers between devices, from_behind(): return lax.ppermute(value, axis, pairs)  35.9 us
    ppermute x4, waiting for transfers between devices, from_behind(): return lax.ppermute(value, axis, pairs)  19.2 us
    dot_general x1, matrix products, body(): up_total = jnp.dot(whole_rows, up_whole, preferred_element_type=jnp.float32)  7.38 us
    dot_general x1, matrix products, body(): jnp.dot(whole_rows, gate_whole, preferred_element_type=jnp.float32)  7.12 us
  transfers between devices with their start and end apart: 13, of which 12 were waited for; matrix products, arithmetic and copies ran while one was open for 17% of the time, Pallas kernels for 0%

commit v1 on v0

--- a/solution.py
+++ b/solution.py
@@ -260,7 +260,20 @@
     down_matrix,
 ):
     gate_whole = lax.all_gather(gate_matrix, "sp", axis=0, tiled=True)
-    up_whole = lax.all_gather(up_matrix, "sp", axis=0, tiled=True)
+
+    def _mix_packet(target, mesh_dim):
+        n_parts = lax.axis_size(mesh_dim)
+        val = sorted(((idx, (idx + 1) % n_parts) for idx in range(n_parts)))
+        left_arr = target
+        by_rank = [left_arr]
+        for to_i in [*range(1, n_parts)]:
+            left_arr = lax.ppermute(left_arr, mesh_dim, val)
+            by_rank.insert(0, left_arr)
+        wide_out = jnp.concatenate(by_rank, 0)
+        x_now = jnp.roll(wide_out, shift=(lax.axis_index(mesh_dim) + 1) * target.shape[0], axis=0)
+        return x_now
+
+    up_whole = _mix_packet(up_matrix, "sp")
     down_whole = lax.all_gather(down_matrix, "sp", axis=1, tiled=True)
     block_outputs, decay_spans, matrix_product, running_state, _ = local_recurrence(
         query_projected,

time: 327 us -> 358 us (1.095)
  matrix products: 55.6 us -> 80.4 us
  waiting for transfers between devices: 212 us -> 191 us
  local copies, waits for them, and re-layouts: 2.49 us -> 18.6 us
  other arithmetic: 3.82 us -> 12.7 us
    ppermute x0 -> x7, waiting for transfers between devices: none -> 163 us  [_mix_packet(): left_arr = lax.ppermute(left_arr, mesh_dim, val)]
    all_gather x1, waiting for transfers between devices: 86 us -> 0.01 us  [body(): down_whole = lax.all_gather(down_matrix, 'sp', axis=1, tiled=True)]
    all_gather x1 -> x0, waiting for transfers between devices: 67.4 us -> none  [body(): up_whole = lax.all_gather(up_matrix, 'sp', axis=0, tiled=True)]
    ppermute x6, waiting for transfers between devices: 37.2 us -> 19.2 us  [swap(): return lax.ppermute(value, axis, [(i, i ^ bit) for i in range(size)])]
    unnamed x37 -> x60, local copies, waits for them, and re-layouts: 0.79 us -> 14.7 us
    ppermute x4, waiting for transfers between devices: 19.2 us -> 8.39 us  [from_behind(): return lax.ppermute(value, axis, pairs)]
    ppermute x4, starting transfers between devices: 35.9 us -> 25.3 us  [from_behind(): return lax.ppermute(value, axis, pairs)]
    ppermute x0 -> x7, starting transfers between devices: none -> 6.88 us  [_mix_packet(): left_arr = lax.ppermute(left_arr, mesh_dim, val)]
  transfers between devices with their start and end apart: 13 -> 19, of which waited for: 12 -> 14; matrix products, arithmetic and copies ran while one was open for 17% -> 28% of each run, Pallas kernels for 0% -> 0%
where the time goes in v1:
time: 358 us; the launch traced here: 355 us
  waiting for transfers between devices  191 us (53%)
  matrix products  80.4 us (22%)
  starting transfers between devices  37.8 us (11%)
  local copies, waits for them, and re-layouts  18.6 us (5%)
  between operations  14.1 us (4%)
  other arithmetic  12.7 us (4%)
    ppermute x7, waiting for transfers between devices, _mix_packet(): left_arr = lax.ppermute(left_arr, mesh_dim, val)  163 us
    ppermute x4, starting transfers between devices, from_behind(): return lax.ppermute(value, axis, pairs)  25.3 us
    ppermute x6, waiting for transfers between devices, swap(): return lax.ppermute(value, axis, [(i, i ^ bit) for i in range(size)])  19.2 us
    unnamed x60, local copies, waits for them, and re-layouts  14.7 us
    dot_general x6, matrix products, advance(): jnp.einsum('hij,hjv->hiv', inner_scores, new_state, precision=PRECISION_F...  10.1 us
    ppermute x4, waiting for transfers between devices, from_behind(): return lax.ppermute(value, axis, pairs)  8.39 us
    dot_general x6, matrix products, advance(): jnp.einsum('xwp,xws->xps', decayed_keys, new_state, precision=PRECISION_F...  7.42 us
    dot_general x6, matrix products, advance(): jnp.einsum('hik,hij->hkj', decayed_keys, householder_weights, precision=P...  7.36 us
  transfers between devices with their start and end apart: 19, of which 14 were waited for; matrix products, arithmetic and copies ran while one was open for 28% of the time, Pallas kernels for 0%

profile of v1, /device:TPU:0, one launch (start us, length us, event | category | flops | bytes accessed | tf_op | source)
XLA Modules:
  0.0 355.4 jit_solution(16551163248404086554)
XLA Ops:
  24.0 51.8 %while.17 = (s32[]{:T(128)}, f32[2,128,128]{2,1,0:T(8,128)S(1)}, f32[2,128,128]{2,1,0:T(8,128)S(1)}, f32[6,2,64,128]{3,2,0,1:T(8,128)}, f32[6,2,64,128]{3,2,0,1:...) while((s32[]{:T(128)}, f32[2,128,128]{2,1,0:T(8,128)S(1)}, ...), condition=%wide.region_4.5_spmd.clone, body=%wide.region_3.4_spmd.clone.sunk | while | flops 201605120 | bytes 2759341 | solution.py:229
  26.3 1.7 fusion.208
  34.9 1.7 fusion.208
  43.5 1.7 fusion.208
  52.1 1.7 fusion.208
  60.7 1.7 fusion.208
  69.4 1.7 fusion.208
  75.9 4.9 %collective-permute-start = (bf16[2,128,256]{2,1,0:T(8,128)(2,1)S(1)}, bf16[2,128,256]{2,1,0:T(8,128)(2,1)S(1)}, u32[]{:S(2)}, u32[]{:S(2)}) collective-permute-start(bf16[2,128,256]{2,1,0:T(8,128)(2,1)S(1)} %pad_maximum_fusion.6), channel_id=1, source_target_pairs={{0,4},{4,8},{8,12},{12,16},{16,20},{20,24},{24,28},{1,5},{5,9},{9,... | collective-permute-start | bytes 393224 | tf_op jit(solution)/shard_map/ppermute | solution.py:15
  80.8 5.3 %collective-permute-done = bf16[2,128,256]{2,1,0:T(8,128)(2,1)S(1)} collective-permute-done((bf16[2,128,256]{2,1,0:T(8,128)(2,1)S(1)}, bf16[2,128,256]{2,1,0:T(8,128)(2,1)S(1)}, u32[]{:S(2)}, u32[]{:S(2)}) %collective-permute-start) | collective-permute-done | bytes 131104 | tf_op jit(solution)/shard_map/ppermute | solution.py:15
  86.1 4.4 %collective-permute-start.1 = (bf16[2,128,256]{2,1,0:T(8,128)(2,1)S(1)}, bf16[2,128,256]{2,1,0:T(8,128)(2,1)S(1)}, u32[]{:S(2)}, u32[]{:S(2)}) collective-permute-start(bf16[2,128,256]{2,1,0:T(8,128)(2,1)S(1)} %collective-permute-done), channel_id=1, source_target_pairs={{0,4},{4,8},{8,12},{12,16},{16,20},{20,24},{24,28},{1,5},{5,9},{9,... | collective-permute-start | bytes 393224 | tf_op jit(solution)/shard_map/ppermute | solution.py:15
  90.5 2.9 collective-permute-start.8
  93.9 10.1 %collective-permute-start.2 = (bf16[2,128,256]{2,1,0:T(8,128)(2,1)S(1)}, bf16[2,128,256]{2,1,0:T(8,128)(2,1)S(1)}, u32[]{:S(2)}, u32[]{:S(2)}) collective-permute-start(bf16[2,128,256]{2,1,0:T(8,128)(2,1)S(1)} %pad_maximum_fusion.7), channel_id=1, source_target_pairs={{0,8},{4,12},{8,16},{12,20},{16,24},{20,28},{1,9},{5,13},{9,17},{1... | collective-permute-start | bytes 393224 | tf_op jit(solution)/shard_map/ppermute | solution.py:15
  104.0 2.5 collective-permute-done.2
  106.8 15.4 %collective-permute-done.8 = bf16[256,1408]{1,0:T(8,128)(2,1)S(1)} collective-permute-done((bf16[256,1408]{1,0:T(8,128)(2,1)S(1)}, bf16[256,1408]{1,0:T(8,128)(2,1)S(1)}, u32[]{:S(2)}, u32[]{:S(2)}) %collective-permute-start.8) | collective-permute-done | bytes 720928 | tf_op jit(solution)/shard_map/ppermute | solution.py:270
  122.3 2.9 collective-permute-start.9
  125.8 5.9 %collective-permute-start.3 = (bf16[2,128,128]{2,1,0:T(8,128)(2,1)}, bf16[2,128,128]{2,1,0:T(8,128)(2,1)}, u32[]{:S(2)}, u32[]{:S(2)}) collective-permute-start(bf16[2,128,128]{2,1,0:T(8,128)(2,1)} %fusion.132), channel_id=1, source_target_pairs={{0,16},{4,20},{8,24},{12,28},{1,17},{5,21},{9,25},{13,29},{2,18},{... | collective-permute-start | bytes 196616 | tf_op jit(solution)/shard_map/ppermute | solution.py:15
  136.2 10.9 %collective-permute-done.9 = bf16[256,1408]{1,0:T(8,128)(2,1)S(1)} collective-permute-done((bf16[256,1408]{1,0:T(8,128)(2,1)S(1)}, bf16[256,1408]{1,0:T(8,128)(2,1)S(1)}, u32[]{:S(2)}, u32[]{:S(2)}) %collective-permute-start.9) | collective-permute-done | bytes 720928 | tf_op jit(solution)/shard_map/ppermute | solution.py:270
  151.3 35.6 %collective-permute-done.10 = bf16[256,1408]{1,0:T(8,128)(2,1)} collective-permute-done((bf16[256,1408]{1,0:T(8,128)(2,1)S(1)}, bf16[256,1408]{1,0:T(8,128)(2,1)}, u32[]{:S(2)}, u32[]{:S(2)}) %collective-permute-start.10) | collective-permute-done | bytes 720928 | tf_op jit(solution)/shard_map/ppermute | solution.py:270
  187.3 34.9 %collective-permute-done.11 = bf16[256,1408]{1,0:T(8,128)(2,1)S(1)} collective-permute-done((bf16[256,1408]{1,0:T(8,128)(2,1)}, bf16[256,1408]{1,0:T(8,128)(2,1)S(1)}, u32[]{:S(2)}, u32[]{:S(2)}) %collective-permute-start.11) | collective-permute-done | bytes 720928 | tf_op jit(solution)/shard_map/ppermute | solution.py:270
  222.7 1.8 collective-permute-start.5
  224.5 33.1 %collective-permute-done.12 = bf16[256,1408]{1,0:T(8,128)(2,1)S(1)} collective-permute-done((bf16[256,1408]{1,0:T(8,128)(2,1)S(1)}, bf16[256,1408]{1,0:T(8,128)(2,1)S(1)}, u32[]{:S(2)}, u32[]{:S(2)}) %collective-permute-start.12) | collective-permute-done | bytes 720928 | tf_op jit(solution)/shard_map/ppermute | solution.py:270
  258.5 25.7 %collective-permute-done.13 = bf16[256,1408]{1,0:T(8,128)(2,1)} collective-permute-done((bf16[256,1408]{1,0:T(8,128)(2,1)S(1)}, bf16[256,1408]{1,0:T(8,128)(2,1)}, u32[]{:S(2)}, u32[]{:S(2)}) %collective-permute-start.13) | collective-permute-done | bytes 720928 | tf_op jit(solution)/shard_map/ppermute | solution.py:270
  285.1 1.7 collective-permute-start.6
  286.8 7.5 %collective-permute-done.6 = bf16[96,2048]{1,0:T(8,128)(2,1)} collective-permute-done((bf16[96,2048]{1,0:T(8,128)(2,1)}, bf16[96,2048]{1,0:T(8,128)(2,1)}, u32[]{:S(2)}, u32[]{:S(2)}) %collective-permute-start.6) | collective-permute-done | bytes 393248 | tf_op jit(solution)/shard_map/ppermute | solution.py:46
  295.5 7.4 %collective-permute-done.14 = bf16[256,1408]{1,0:T(8,128)(2,1)} collective-permute-done((bf16[256,1408]{1,0:T(8,128)(2,1)}, bf16[256,1408]{1,0:T(8,128)(2,1)}, u32[]{:S(2)}, u32[]{:S(2)}) %collective-permute-start.14) | collective-permute-done | bytes 720928 | tf_op jit(solution)/shard_map/ppermute | solution.py:270
  312.3 4.3 %copy-done.16 = bf16[4096,1408]{1,0:T(8,128)(2,1)} copy-done((bf16[4096,1408]{1,0:T(8,128)(2,1)}, bf16[4096,1408]{1,0:T(8,128)(2,1)S(1)}, u32[]{:S(2)}) %copy-start.16) | copy-done | bytes 11534360
  316.5 5.8 %fusion.48 = f32[384,1408]{1,0:T(8,128)S(1)} fusion(bf16[2048,1408]{1,0:T(8,128)(2,1)} %all-gather.3.cloned.1.call-done, bf16[192,2048]{1,0:T(8,128)(2,1)} %collective-permute-done.7, bf16[96,2048]{1,0:T(8,128)(2,1)} %collective-permute-done.6, bf16[96,2048]{1,0:T(8,128)(2,1)} %multiply_convert_fusion.1), kind=kOutput, calls=%fused_computation.76 | convolution fusion | flops 2219311104 | bytes 9502720 | tf_op jit(solution)/shard_map/dot_general | solution.py:310
  322.9 5.1 %multiply_convert_fusion = bf16[384,1408]{1,0:T(8,128)(2,1)} fusion(f32[384,1408]{1,0:T(8,128)S(1)} %fusion.48, bf16[4096,1408]{1,0:T(8,128)(2,1)S(1)} %copy-done.17, s32[]{:T(128)S(6)} %select_n.205, bf16[192,2048]{1,0:T(8,128)(2,1)} %collective-permute-done.7, bf16[96,2048]{1,0:T(8,128)(2,1)} %collective-permute-done.6, ...), kind=kOutput, calls=%fused_computation.48 | convolution fusion | flops 2222555136 | bytes 10584068 | tf_op jit(solution)/shard_map/dot_general | solution.py:311
  328.0 4.3 %convolution_convert_fusion = bf16[192,2048]{1,0:T(8,128)(2,1)S(1)} fusion(bf16[1408,2048]{1,0:T(8,128)(2,1)} %all-gather.5.cloned.1.call-done, bf16[384,1408]{1,0:T(8,128)(2,1)} %multiply_convert_fusion), kind=kOutput, calls=%fused_computation.46 | convolution fusion | flops 1107689472 | bytes 7094272 | tf_op jit(solution)/shard_map/dot_general | solution.py:71
  332.5 2.3 collective-permute-done.15
  336.2 1.9 collective-permute-start.16
  338.1 9.4 %collective-permute-done.16 = bf16[96,2048]{1,0:T(8,128)(2,1)S(1)} collective-permute-done((bf16[96,2048]{1,0:T(8,128)(2,1)S(1)}, bf16[96,2048]{1,0:T(8,128)(2,1)S(1)}, u32[]{:S(2)}, u32[]{:S(2)}) %collective-permute-start.16) | collective-permute-done | bytes 393248 | tf_op jit(solution)/shard_map/ppermute | solution.py:46
  (202 shorter events, 84.7 us)
Async XLA Ops:
  6.5 180.3 %copy-start = (bf16[256,2048]{1,0:T(8,128)(2,1)S(1)}, bf16[256,2048]{1,0:T(8,128)(2,1)}, u32[]{:S(2)}) copy-start(bf16[256,2048]{1,0:T(8,128)(2,1)} %param.27) | copy-start | bytes 3145732
  6.5 310.0 %all-gather.3.cloned.1.call-start = ((), (), s32[]{:S(2)}) async-start(), calls=%async_computation | async-start | bytes 6488064 | tf_op jit(solution)/shard_map/all_gather | solution.py:262
  7.3 320.8 %all-gather.5.cloned.1.call-start = ((), (), s32[]{:S(2)}) async-start(), calls=%async_computation.1 | async-start | bytes 6488064 | tf_op jit(solution)/shard_map/all_gather | solution.py:277
  24.0 66.5 %copy-start.2 = (bf16[256,1408]{1,0:T(8,128)(2,1)S(1)}, bf16[256,1408]{1,0:T(8,128)(2,1)}, u32[]{:S(2)}) copy-start(bf16[256,1408]{1,0:T(8,128)(2,1)} %param.30) | copy-start | bytes 2162692
  75.8 72.4 %copy-start.19 = (f32[128]{0:T(128)S(1)}, f32[128]{0:T(128)}, u32[]{:S(2)}) copy-start(f32[128]{0:T(128)} %param.26) | copy-start | bytes 1540
  75.9 10.2 %collective-permute-start = (bf16[2,128,256]{2,1,0:T(8,128)(2,1)S(1)}, bf16[2,128,256]{2,1,0:T(8,128)(2,1)S(1)}, u32[]{:S(2)}, u32[]{:S(2)}) collective-permute-start(bf16[2,128,256]{2,1,0:T(8,128)(2,1)S(1)} %pad_maximum_fusion.6), channel_id=1, source_target_pairs={{0,4},{4,8},{8,12},{12,16},{16,20},{20,24},{24,28},{1,5},{5,9},{9,... | collective-permute-start | bytes 393224 | tf_op jit(solution)/shard_map/ppermute | solution.py:15
  86.1 45.7 %copy-start.14 = (bf16[2,128,256]{2,1,0:T(8,128)(2,1)}, bf16[2,128,256]{2,1,0:T(8,128)(2,1)S(1)}, u32[]{:S(2)}) copy-start(bf16[2,128,256]{2,1,0:T(8,128)(2,1)S(1)} %collective-permute-done) | copy-start | bytes 393220
  86.1 7.6 %collective-permute-start.1 = (bf16[2,128,256]{2,1,0:T(8,128)(2,1)S(1)}, bf16[2,128,256]{2,1,0:T(8,128)(2,1)S(1)}, u32[]{:S(2)}, u32[]{:S(2)}) collective-permute-start(bf16[2,128,256]{2,1,0:T(8,128)(2,1)S(1)} %collective-permute-done), channel_id=1, source_target_pairs={{0,4},{4,8},{8,12},{12,16},{16,20},{20,24},{24,28},{1,5},{5,9},{9,... | collective-permute-start | bytes 393224 | tf_op jit(solution)/shard_map/ppermute | solution.py:15
  90.5 31.8 %collective-permute-start.8 = (bf16[256,1408]{1,0:T(8,128)(2,1)S(1)}, bf16[256,1408]{1,0:T(8,128)(2,1)S(1)}, u32[]{:S(2)}, u32[]{:S(2)}) collective-permute-start(bf16[256,1408]{1,0:T(8,128)(2,1)S(1)} %copy-done.2), channel_id=1, source_target_pairs={{0,4},{4,8},{8,12},{12,16},{16,20},{20,24},{24,28},{28,0},{1,5},{5... | collective-permute-start | bytes 2162696 | tf_op jit(solution)/shard_map/ppermute | solution.py:270
  93.9 12.6 %collective-permute-start.2 = (bf16[2,128,256]{2,1,0:T(8,128)(2,1)S(1)}, bf16[2,128,256]{2,1,0:T(8,128)(2,1)S(1)}, u32[]{:S(2)}, u32[]{:S(2)}) collective-permute-start(bf16[2,128,256]{2,1,0:T(8,128)(2,1)S(1)} %pad_maximum_fusion.7), channel_id=1, source_target_pairs={{0,8},{4,12},{8,16},{12,20},{16,24},{20,28},{1,9},{5,13},{9,17},{1... | collective-permute-start | bytes 393224 | tf_op jit(solution)/shard_map/ppermute | solution.py:15
  106.8 25.0 %copy-start.12 = (f32[2,128,256]{2,1,0:T(8,128)}, f32[2,128,256]{2,1,0:T(8,128)S(1)}, u32[]{:S(2)}) copy-start(f32[2,128,256]{2,1,0:T(8,128)S(1)} %fusion.96) | copy-start | bytes 786436
  122.3 100.0 %copy-start.4 = (bf16[256,1408]{1,0:T(8,128)(2,1)}, bf16[256,1408]{1,0:T(8,128)(2,1)S(1)}, u32[]{:S(2)}) copy-start(bf16[256,1408]{1,0:T(8,128)(2,1)S(1)} %collective-permute-done.8) | copy-start | bytes 2162692
  122.3 24.9 %collective-permute-start.9 = (bf16[256,1408]{1,0:T(8,128)(2,1)S(1)}, bf16[256,1408]{1,0:T(8,128)(2,1)S(1)}, u32[]{:S(2)}, u32[]{:S(2)}) collective-permute-start(bf16[256,1408]{1,0:T(8,128)(2,1)S(1)} %collective-permute-done.8), channel_id=1, source_target_pairs={{0,4},{4,8},{8,12},{12,16},{16,20},{20,24},{24,28},{28,0},{1,5},{5... | collective-permute-start | bytes 2162696 | tf_op jit(solution)/shard_map/ppermute | solution.py:270
  125.8 7.5 %collective-permute-start.3 = (bf16[2,128,128]{2,1,0:T(8,128)(2,1)}, bf16[2,128,128]{2,1,0:T(8,128)(2,1)}, u32[]{:S(2)}, u32[]{:S(2)}) collective-permute-start(bf16[2,128,128]{2,1,0:T(8,128)(2,1)} %fusion.132), channel_id=1, source_target_pairs={{0,16},{4,20},{8,24},{12,28},{1,17},{5,21},{9,25},{13,29},{2,18},{... | collective-permute-start | bytes 196616 | tf_op jit(solution)/shard_map/ppermute | solution.py:15
  131.8 125.8 %copy-start.1 = (bf16[96,2048]{1,0:T(8,128)(2,1)S(1)}, bf16[96,2048]{1,0:T(8,128)(2,1)}, u32[]{:S(2)}) copy-start(bf16[96,2048]{1,0:T(8,128)(2,1)} %param.17) | copy-start | bytes 1179652
  134.5 149.6 %copy-start.18 = (f32[2048]{0:T(1024)S(1)}, f32[2048]{0:T(1024)}, u32[]{:S(2)}) copy-start(f32[2048]{0:T(1024)} %param.28) | copy-start | bytes 24580
  147.1 75.1 %copy-start.6 = (bf16[256,1408]{1,0:T(8,128)(2,1)}, bf16[256,1408]{1,0:T(8,128)(2,1)S(1)}, u32[]{:S(2)}) copy-start(bf16[256,1408]{1,0:T(8,128)(2,1)S(1)} %collective-permute-done.9) | copy-start | bytes 2162692
  147.1 39.7 %collective-permute-start.10 = (bf16[256,1408]{1,0:T(8,128)(2,1)S(1)}, bf16[256,1408]{1,0:T(8,128)(2,1)}, u32[]{:S(2)}, u32[]{:S(2)}) collective-permute-start(bf16[256,1408]{1,0:T(8,128)(2,1)S(1)} %collective-permute-done.9), channel_id=1, source_target_pairs={{0,4},{4,8},{8,12},{12,16},{16,20},{20,24},{24,28},{28,0},{1,5},{5... | collective-permute-start | bytes 2162696 | tf_op jit(solution)/shard_map/ppermute | solution.py:270
  186.8 35.4 %collective-permute-start.11 = (bf16[256,1408]{1,0:T(8,128)(2,1)}, bf16[256,1408]{1,0:T(8,128)(2,1)S(1)}, u32[]{:S(2)}, u32[]{:S(2)}) collective-permute-start(bf16[256,1408]{1,0:T(8,128)(2,1)} %collective-permute-done.10), channel_id=1, source_target_pairs={{0,4},{4,8},{8,12},{12,16},{16,20},{20,24},{24,28},{28,0},{1,5},{5... | collective-permute-start | bytes 2162696 | tf_op jit(solution)/shard_map/ppermute | solution.py:270
  187.2 35.0 %collective-permute-start.4 = (bf16[192,2048]{1,0:T(8,128)(2,1)S(1)}, bf16[192,2048]{1,0:T(8,128)(2,1)S(1)}, u32[]{:S(2)}, u32[]{:S(2)}) collective-permute-start(bf16[192,2048]{1,0:T(8,128)(2,1)S(1)} %convolution_convert_fusion.1), channel_id=1, source_target_pairs={{0,1},{1,0},{2,3},{3,2},{4,5},{5,4},{6,7},{7,6},{8,9},{9,8},{10,11... | collective-permute-start | bytes 2359304 | tf_op jit(solution)/shard_map/ppermute | solution.py:46
  222.2 35.4 %copy-start.8 = (bf16[256,1408]{1,0:T(8,128)(2,1)}, bf16[256,1408]{1,0:T(8,128)(2,1)S(1)}, u32[]{:S(2)}) copy-start(bf16[256,1408]{1,0:T(8,128)(2,1)S(1)} %collective-permute-done.11) | copy-start | bytes 2162692
  222.2 35.4 %collective-permute-start.12 = (bf16[256,1408]{1,0:T(8,128)(2,1)S(1)}, bf16[256,1408]{1,0:T(8,128)(2,1)S(1)}, u32[]{:S(2)}, u32[]{:S(2)}) collective-permute-start(bf16[256,1408]{1,0:T(8,128)(2,1)S(1)} %collective-permute-done.11), channel_id=1, source_target_pairs={{0,4},{4,8},{8,12},{12,16},{16,20},{20,24},{24,28},{28,0},{1,5},{5... | collective-permute-start | bytes 2162696 | tf_op jit(solution)/shard_map/ppermute | solution.py:270
  222.7 34.9 %collective-permute-start.5 = (bf16[96,2048]{1,0:T(8,128)(2,1)S(1)}, bf16[96,2048]{1,0:T(8,128)(2,1)S(1)}, u32[]{:S(2)}, u32[]{:S(2)}) collective-permute-start(bf16[96,2048]{1,0:T(8,128)(2,1)S(1)} %slice.148), channel_id=1, source_target_pairs={{0,2},{1,3},{2,0},{3,1},{4,6},{5,7},{6,4},{7,5},{8,10},{9,11},{10,... | collective-permute-start | bytes 1179656 | tf_op jit(solution)/shard_map/ppermute | solution.py:46
  257.6 26.5 %collective-permute-start.13 = (bf16[256,1408]{1,0:T(8,128)(2,1)S(1)}, bf16[256,1408]{1,0:T(8,128)(2,1)}, u32[]{:S(2)}, u32[]{:S(2)}) collective-permute-start(bf16[256,1408]{1,0:T(8,128)(2,1)S(1)} %collective-permute-done.12), channel_id=1, source_target_pairs={{0,4},{4,8},{8,12},{12,16},{16,20},{20,24},{24,28},{28,0},{1,5},{5... | collective-permute-start | bytes 2162696 | tf_op jit(solution)/shard_map/ppermute | solution.py:270
  284.1 18.8 %collective-permute-start.14 = (bf16[256,1408]{1,0:T(8,128)(2,1)}, bf16[256,1408]{1,0:T(8,128)(2,1)}, u32[]{:S(2)}, u32[]{:S(2)}) collective-permute-start(bf16[256,1408]{1,0:T(8,128)(2,1)} %collective-permute-done.13), channel_id=1, source_target_pairs={{0,4},{4,8},{8,12},{12,16},{16,20},{20,24},{24,28},{28,0},{1,5},{5... | collective-permute-start | bytes 2162696 | tf_op jit(solution)/shard_map/ppermute | solution.py:270
  285.1 9.2 %collective-permute-start.6 = (bf16[96,2048]{1,0:T(8,128)(2,1)}, bf16[96,2048]{1,0:T(8,128)(2,1)}, u32[]{:S(2)}, u32[]{:S(2)}) collective-permute-start(bf16[96,2048]{1,0:T(8,128)(2,1)} %multiply_convert_fusion.1), channel_id=1, source_target_pairs={{0,2},{1,3},{2,0},{3,1},{4,6},{5,7},{6,4},{7,5},{8,10},{9,11},{10,... | collective-permute-start | bytes 1179656 | tf_op jit(solution)/shard_map/ppermute | solution.py:46
  286.7 21.1 %copy-start.7 = (bf16[256,1408]{1,0:T(8,128)(2,1)S(1)}, bf16[256,1408]{1,0:T(8,128)(2,1)}, u32[]{:S(2)}) copy-start(bf16[256,1408]{1,0:T(8,128)(2,1)} %copy-done.6) | copy-start | bytes 2162692
  286.7 21.2 %copy-start.5 = (bf16[256,1408]{1,0:T(8,128)(2,1)S(1)}, bf16[256,1408]{1,0:T(8,128)(2,1)}, u32[]{:S(2)}) copy-start(bf16[256,1408]{1,0:T(8,128)(2,1)} %copy-done.4) | copy-start | bytes 2162692
  286.7 21.3 %copy-start.3 = (bf16[256,1408]{1,0:T(8,128)(2,1)S(1)}, bf16[256,1408]{1,0:T(8,128)(2,1)}, u32[]{:S(2)}) copy-start(bf16[256,1408]{1,0:T(8,128)(2,1)} %param.30) | copy-start | bytes 2162692
  295.4 21.1 %collective-permute-start.7 = (bf16[192,2048]{1,0:T(8,128)(2,1)S(1)}, bf16[192,2048]{1,0:T(8,128)(2,1)}, u32[]{:S(2)}, u32[]{:S(2)}) collective-permute-start(bf16[192,2048]{1,0:T(8,128)(2,1)S(1)} %pad_maximum_fusion.1), channel_id=1, source_target_pairs={{0,1},{1,0},{2,3},{3,2},{4,5},{5,4},{6,7},{7,6},{8,9},{9,8},{10,11... | collective-permute-start | bytes 2359304 | tf_op jit(solution)/shard_map/ppermute | solution.py:46
  332.4 2.4 collective-permute-start.15
  336.2 11.4 %collective-permute-start.16 = (bf16[96,2048]{1,0:T(8,128)(2,1)S(1)}, bf16[96,2048]{1,0:T(8,128)(2,1)S(1)}, u32[]{:S(2)}, u32[]{:S(2)}) collective-permute-start(bf16[96,2048]{1,0:T(8,128)(2,1)S(1)} %slice.147), channel_id=1, source_target_pairs={{0,2},{1,3},{2,0},{3,1},{4,6},{5,7},{6,4},{7,5},{8,10},{9,11},{10,... | collective-permute-start | bytes 1179656 | tf_op jit(solution)/shard_map/ppermute | solution.py:46
  (9 other events, 60.8 us)
Sparse Core Ops, SparseCore 0:
  9.5 96.1 all-gather.2
  131.9 132.9 all-gather.4
